TPU v7x, 32 devices: a whole 2x2x4 slice. The times are simulated.
32 devices in a mesh: fs: 16 (over z, y, core), tp: 2 (over x).
Axes of the slice: x: 2, y: 2, z: 4, core: 2. Of those that a mesh axis runs over, the one named last changes fastest.
Arguments:
- tokens: bfloat16 [4096, 2048], P('fs', 'tp'), may hold values from -16 to 16, as said below
- mix_gain: bfloat16 [2048], P('tp'), may hold values from 0.099609375 to 1.8984375
- query_weight: bfloat16 [2048, 512], P('fs', 'tp'), may hold values from -0.125 to 0.125
- key_weight: bfloat16 [2048, 512], P('fs', 'tp'), may hold values from -0.125 to 0.125
- value_weight: bfloat16 [2048, 1024], P('fs', 'tp'), may hold values from -0.125 to 0.125
- output_gate_weight: bfloat16 [2048, 1024], P('fs', 'tp'), may hold values from -0.125 to 0.125
- out_weight: bfloat16 [1024, 2048], P('tp', 'fs'), may hold values from -0.1875 to 0.1875
- head_rates: float32 [8], P('tp'), may hold values from 0 to 1, as said below
- block_scale: float32 [32], P('fs'), may hold values from 0.5 to 2
- ffn_gain: bfloat16 [2048], P('tp'), may hold values from 0.099609375 to 1.8984375
- ff_gate: bfloat16 [2048, 5632], P('fs', 'tp'), may hold values from -0.125 to 0.125
- ff_up: bfloat16 [2048, 5632], P('fs', 'tp'), may hold values from -0.125 to 0.125
- ff_down: bfloat16 [5632, 2048], P('tp', 'fs'), may hold values from -0.078125 to 0.078125
- final_gain: bfloat16 [2048], P('tp'), may hold values from 0.099609375 to 1.8984375
Outputs:
- layer_out: bfloat16 [4096, 2048], P('fs', 'tp')
Inputs may be any that keep to these rules, and one draw needn't show every extreme that they name: `tokens`: column blocks of the activations have different scales. `head_rates`: positive rates.
All inputs are finite; a program needn't handle non-finite values.
Results may differ from a plain program's by a relative error of at most 0.014.
Values may be sent and summed in bfloat16 or wider, within the bound.
A program may use at most 128 MiB of HBM per device.

v0:
```python
import jax
import jax.numpy as jnp
from jax import lax
from jax.sharding import PartitionSpec as P

D = 2048
DK = 64
DV = 128
BLK = 128
SEQ_LEN = 256
EPS = 1e-06
THETA = 10000.0


def rms_norm(values, gain):
    scale = lax.rsqrt(jnp.mean(values * values, axis=-1, keepdims=True) + EPS)
    return values * scale * gain.astype(jnp.float32)


def rotate(values, positions):
    half = values.shape[-1] // 2
    inverse = THETA ** (-jnp.arange(half, dtype=jnp.float32) / half)
    angle = positions.astype(jnp.float32)[:, None] * inverse
    cosine = jnp.cos(angle)[:, None, :]
    sine = jnp.sin(angle)[:, None, :]
    first = values[..., :half]
    second = values[..., half:]
    return jnp.concatenate(
        [first * cosine - second * sine, second * cosine + first * sine], axis=-1
    )


def retain(query, key, value, rates, scales):
    rows, heads_here, width_k = query.shape
    width_v = value.shape[-1]
    nblk = rows // BLK
    hi = lax.Precision.HIGHEST
    qblk = query.astype(jnp.float32).reshape(nblk, BLK, heads_here, width_k)
    kblk = key.astype(jnp.float32).reshape(nblk, BLK, heads_here, width_k)
    vblk = value.astype(jnp.float32).reshape(nblk, BLK, heads_here, width_v)
    logdec = -rates[None, :] * scales[:, None]
    steps = jnp.arange(BLK, dtype=jnp.float32)
    offset = steps[:, None] - steps[None, :]
    causal = offset >= 0
    inside = jnp.where(
        causal[None, None],
        jnp.exp(logdec[:, :, None, None] * jnp.where(causal, offset, 0.0)[None, None]),
        0.0,
    )
    scores = jnp.einsum("nchd,nmhd->nhcm", qblk, kblk, precision=hi) * inside
    inner = jnp.einsum("nhcm,nmhe->nche", scores, vblk, precision=hi)
    zeta = jnp.exp(logdec[:, :, None] * (BLK - 1.0 - steps)[None, None, :])
    kv_block = jnp.einsum(
        "nchd,nche->nhde", kblk * jnp.transpose(zeta, (0, 2, 1))[..., None], vblk, precision=hi
    )
    hold = jnp.exp(logdec * BLK)
    per_seq = SEQ_LEN // BLK
    fresh = (jnp.arange(nblk, dtype=jnp.int32) % per_seq == 0).astype(jnp.float32)

    def advance(state, inputs):
        kv_now, hold_now, fresh_now = inputs
        before = state * (1.0 - fresh_now)
        return (before * hold_now[:, None, None] + kv_now, before)

    start = jnp.zeros((heads_here, width_k, width_v), jnp.float32)
    _, before = lax.scan(advance, start, (kv_block, hold, fresh))
    xi = jnp.exp(logdec[:, :, None] * (steps + 1.0)[None, None, :])
    cross = jnp.einsum(
        "nchd,nhde->nche", qblk * jnp.transpose(xi, (0, 2, 1))[..., None], before, precision=hi
    )
    total = inner + cross
    total = total * lax.rsqrt(jnp.mean(total * total, axis=-1, keepdims=True) + EPS)
    return total.reshape(rows, heads_here * width_v)


def fold_maker(source, pieces):
    return tuple((jnp.dot(source, piece, preferred_element_type=jnp.float32) for piece in pieces))


def body(
    tokens,
    mix_gain,
    query_weight,
    key_weight,
    value_weight,
    output_gate_weight,
    out_weight,
    head_rates,
    block_scale,
    ffn_gain,
    ff_gate,
    ff_up,
    ff_down,
    final_gain,
):
    rows = tokens.shape[0]
    heads_here = head_rates.shape[0]
    groups = lax.axis_size("tp")
    positions = jnp.arange(rows, dtype=jnp.int32) % SEQ_LEN
    whole, gain_whole = (
        lax.all_gather(tokens, "tp", axis=1, tiled=True),
        lax.all_gather(mix_gain, "tp", axis=0, tiled=True),
    )
    normed = rms_norm(whole.astype(jnp.float32), gain_whole).astype(jnp.bfloat16)
    qproj, kproj, vproj, gproj = fold_maker(
        normed,
        (
            lax.all_gather(query_weight, "fs", axis=0, tiled=True),
            lax.all_gather(key_weight, "fs", axis=0, tiled=True),
            lax.all_gather(value_weight, "fs", axis=0, tiled=True),
            lax.all_gather(output_gate_weight, "fs", axis=0, tiled=True),
        ),
    )
    query = rotate(qproj.reshape(rows, heads_here, DK), positions).astype(jnp.bfloat16)
    key = (rotate(kproj.reshape(rows, heads_here, DK), positions) * DK ** (-0.5)).astype(
        jnp.bfloat16
    )
    value = vproj.astype(jnp.bfloat16).reshape(rows, heads_here, DV)
    normret = retain(query, key, value, head_rates, block_scale)
    gated = (normret * jax.nn.silu(gproj)).astype(jnp.bfloat16)
    all_heads = lax.all_gather(gated, "tp", axis=1, tiled=True)
    head_rows = lax.all_gather(out_weight, "fs", axis=1, tiled=True)
    feature_block = lax.all_to_all(head_rows, "tp", split_axis=1, concat_axis=0, tiled=True)
    width = all_heads.shape[1] // groups
    left = all_heads.reshape(rows, groups, width)
    right = feature_block.reshape(groups, width, feature_block.shape[1])
    partial_sums = jnp.einsum(
        "rng,nge->nre", left, right, preferred_element_type=jnp.float32
    ).astype(jnp.bfloat16)
    mix = jnp.sum(partial_sums.astype(jnp.float32), axis=0)
    resid = (tokens.astype(jnp.float32) + mix).astype(jnp.bfloat16)
    whole2, gain2 = (
        lax.all_gather(resid, "tp", axis=1, tiled=True),
        lax.all_gather(ffn_gain, "tp", axis=0, tiled=True),
    )
    normed2 = rms_norm(whole2.astype(jnp.float32), gain2).astype(jnp.bfloat16)
    gate_part, up_part = fold_maker(
        normed2,
        (
            lax.all_gather(ff_gate, "fs", axis=0, tiled=True),
            lax.all_gather(ff_up, "fs", axis=0, tiled=True),
        ),
    )
    hidden = (jax.nn.silu(gate_part) * up_part).astype(jnp.bfloat16)
    down_terms = jnp.dot(
        hidden,
        lax.all_gather(ff_down, "fs", axis=1, tiled=True),
        preferred_element_type=jnp.float32,
    )
    ffn = lax.psum_scatter(
        down_terms.astype(jnp.bfloat16), "tp", scatter_dimension=1, tiled=True
    ).astype(jnp.float32)
    total = resid.astype(jnp.float32) + ffn
    squares = lax.psum(jnp.sum(total * total, axis=-1, keepdims=True), "tp")
    scale = lax.rsqrt(squares / D + EPS)
    return (total * scale * final_gain.astype(jnp.float32)).astype(jnp.bfloat16)


def solution(mesh):
    return jax.shard_map(
        body,
        mesh=mesh,
        in_specs=(
            P("fs", "tp"),
            P("tp"),
            P("fs", "tp"),
            P("fs", "tp"),
            P("fs", "tp"),
            P("fs", "tp"),
            P("tp", "fs"),
            P("tp"),
            P("fs"),
            P("tp"),
            P("fs", "tp"),
            P("fs", "tp"),
            P("tp", "fs"),
            P("tp"),
        ),
        out_specs=P("fs", "tp"),
        check_vma=False,
    )
```

profile of v0, /device:TPU:0, one launch (start us, length us, event | category | flops | bytes accessed | tf_op | source)
XLA Modules:
  0.0 610.0 jit_solution(6676572417993278447)
XLA Ops:
  6.5 0.7 all-gather.11.cloned.1.call-update
  7.3 0.7 all-gather.15.cloned.1.call-update
  8.1 0.7 all-gather.17.cloned.1.call-update
  8.8 0.5 all-gather.13.cloned.1.call-update
  9.4 1.7 copy.40
  11.1 0.5 all-gather.19.cloned.1.call-update
  11.8 5.5 all_gather.40
  17.3 0.7 neg.35
  18.1 0.7 multiply_exponential_fusion.2
  18.9 14.0 %all-gather.11.cloned.1.call-done = bf16[256,2048]{1,0:T(8,128)(2,1)} async-done(((bf16[256,1024]{1,0:T(8,128)(2,1)}), bf16[256,2048]{1,0:T(8,128)(2,1)}) %all-gather.11.cloned.1.call-update) | async-done | bytes 1048592 | tf_op jit(solution)/shard_map/all_gather | solution.py:101
  32.9 1.6 fusion.2
  34.5 38.5 %all-gather.15.cloned.1.call-done = bf16[2048,256]{1,0:T(8,128)(2,1)} async-done(((bf16[128,256]{1,0:T(8,128)(2,1)}), bf16[2048,256]{1,0:T(8,128)(2,1)}) %all-gather.15.cloned.1.call-update) | async-done | bytes 1048592 | tf_op jit(solution)/shard_map/all_gather | solution.py:108
  73.0 2.2 fusion.50
  75.2 36.8 %all-gather.17.cloned.1.call-done = bf16[2048,256]{1,0:T(8,128)(2,1)} async-done(((bf16[128,256]{1,0:T(8,128)(2,1)}), bf16[2048,256]{1,0:T(8,128)(2,1)}) %all-gather.17.cloned.1.call-update) | async-done | bytes 1048592 | tf_op jit(solution)/shard_map/all_gather | solution.py:109
  112.0 1.9 fusion.48
  114.1 1.1 convolution_multiply_fusion.1
  115.1 39.3 %all-gather.13.cloned.1.call-done = bf16[2048,512]{1,0:T(8,128)(2,1)} async-done(((bf16[128,512]{1,0:T(8,128)(2,1)}), bf16[2048,512]{1,0:T(8,128)(2,1)}) %all-gather.13.cloned.1.call-update) | async-done | bytes 2097168 | tf_op jit(solution)/shard_map/all_gather | solution.py:110
  154.5 2.3 convolution_convert_fusion.1
  156.9 39.8 %all-gather.21.cloned.1.call-done = bf16[512,2048]{0,1:T(8,128)(2,1)} async-done(((bf16[512,128]{0,1:T(8,128)(2,1)}), bf16[512,2048]{0,1:T(8,128)(2,1)}) %all-gather.21.cloned.1.call-update) | async-done | bytes 2097168 | tf_op jit(solution)/shard_map/all_gather | solution.py:122
  196.7 3.9 copy.41
  200.6 3.8 all-to-all-start
  204.8 1.8 fusion.29
  206.5 4.0 while.13
  206.5 0.6 dynamic_slice.24
  207.8 0.7 bitcast_dynamic-update-slice_fusion.4
  208.6 0.6 dynamic_slice.24
  209.8 0.7 bitcast_dynamic-update-slice_fusion.4
  210.6 2.0 multiply_reduce_fusion.1
  212.9 26.1 %all-gather.19.cloned.1.call-done = bf16[2048,512]{1,0:T(8,128)(2,1)} async-done(((bf16[128,512]{1,0:T(8,128)(2,1)}), bf16[2048,512]{1,0:T(8,128)(2,1)}) %all-gather.19.cloned.1.call-update) | async-done | bytes 2097168 | tf_op jit(solution)/shard_map/all_gather | solution.py:111
  238.9 2.8 fusion.16
  241.7 9.2 %all_gather.45 = bf16[256,1024]{1,0:T(8,128)(2,1)S(1)} all-gather(bf16[256,512]{1,0:T(8,128)(2,1)S(1)} %fusion.16), channel_id=1, replica_groups=mesh['fs'=16,'tp'=2] {'tp'}, dimensions={1}, use_global_device_ids=true | all-gather | bytes 786432 | tf_op jit(solution)/shard_map/all_gather | solution.py:121
  251.0 0.7 convert_reduce_fusion
  251.7 1.0 add_convert_fusion
  252.7 0.7 all-gather.25.cloned.1.call-update
  253.5 0.7 all-gather.27.cloned.1.call-update
  254.2 0.5 all-gather.29.cloned.1.call-update
  254.8 4.5 all_gather.48
  259.4 13.5 %all-gather.23.cloned.1.call-done = bf16[256,2048]{1,0:T(8,128)(2,1)} async-done(((bf16[256,1024]{1,0:T(8,128)(2,1)}), bf16[256,2048]{1,0:T(8,128)(2,1)}) %all-gather.23.cloned.1.call-update) | async-done | bytes 1048592 | tf_op jit(solution)/shard_map/all_gather | solution.py:133
  272.8 1.5 fusion.5
  274.4 94.8 %all-gather.25.cloned.1.call-done = bf16[2048,2816]{1,0:T(8,128)(2,1)} async-done(((bf16[128,2816]{1,0:T(8,128)(2,1)}), bf16[2048,2816]{1,0:T(8,128)(2,1)}) %all-gather.25.cloned.1.call-update) | async-done | bytes 11534352 | tf_op jit(solution)/shard_map/all_gather | solution.py:140
  369.1 9.4 %fusion.21 = f32[256,2816]{1,0:T(8,128)} fusion(bf16[2048,2816]{1,0:T(8,128)(2,1)} %all-gather.25.cloned.1.call-done, bf16[256,2048]{1,0:T(8,128)(2,1)} %all-gather.23.cloned.1.call-done, f32[2048]{0:T(1024)S(1)} %convert_element_type.112, f32[256]{0:T(256)S(1)} %add_rsqrt_fusion.2), kind=kOutput, calls=%fused_computation.35 | convolution fusion | flops 2954887168 | bytes 15475712 | tf_op jit(solution)/shard_map/dot_general | solution.py:77
  378.6 85.1 %all-gather.27.cloned.1.call-done = bf16[2048,2816]{1,0:T(8,128)(2,1)} async-done(((bf16[128,2816]{1,0:T(8,128)(2,1)}), bf16[2048,2816]{1,0:T(8,128)(2,1)}) %all-gather.27.cloned.1.call-update) | async-done | bytes 11534352 | tf_op jit(solution)/shard_map/all_gather | solution.py:141
  463.7 97.2 %all-gather.29.cloned.1.call-done = bf16[2816,2048]{1,0:T(8,128)(2,1)} async-done(((bf16[2816,128]{1,0:T(8,128)(2,1)}), bf16[2816,2048]{1,0:T(8,128)(2,1)}) %all-gather.29.cloned.1.call-update) | async-done | bytes 11534352 | tf_op jit(solution)/shard_map/all_gather | solution.py:147
  560.9 15.6 %convolution_convert_fusion = bf16[256,2048]{1,0:T(8,128)(2,1)} fusion(bf16[2816,2048]{1,0:T(8,128)(2,1)} %all-gather.29.cloned.1.call-done, bf16[2048,2816]{1,0:T(8,128)(2,1)} %all-gather.27.cloned.1.call-done, f32[256,2816]{1,0:T(8,128)} %fusion.21, bf16[256,2048]{1,0:T(8,128)(2,1)S(1)} %copy-done.3, f32[2048]{0:T(1024)S(1)} %convert_element_type.112, ...), kind=kOutput, calls=%fused_computation.11 | convolution fusion | flops 5912526848 | bytes 28058624 | tf_op jit(solution)/shard_map/dot_general | solution.py:145
  576.5 18.7 %reduce-scatter.2.cloned.1.call-done = bf16[256,1024]{1,0:T(8,128)(2,1)} async-done(((bf16[256,2048]{1,0:T(8,128)(2,1)}), bf16[256,1024]{1,0:T(8,128)(2,1)}) %reduce-scatter.2.cloned.1.call-update) | async-done | bytes 524304 | tf_op jit(solution)/shard_map/reduce_scatter | solution.py:150
  595.2 1.3 multiply_reduce_fusion
  596.5 4.9 psum.7
  601.4 2.0 multiply_convert_fusion
  (56 shorter events, 1.9 us)
Async XLA Ops:
  6.5 26.4 %all-gather.11.cloned.1.call-start = ((), (), s32[]{:S(2)}) async-start(), calls=%async_computation.2 | async-start | bytes 1572864 | tf_op jit(solution)/shard_map/all_gather | solution.py:101
  7.3 65.7 %all-gather.15.cloned.1.call-start = ((), (), s32[]{:S(2)}) async-start(), calls=%async_computation.4 | async-start | bytes 1114112 | tf_op jit(solution)/shard_map/all_gather | solution.py:108
  8.0 104.0 %all-gather.17.cloned.1.call-start = ((), (), s32[]{:S(2)}) async-start(), calls=%async_computation.5 | async-start | bytes 1114112 | tf_op jit(solution)/shard_map/all_gather | solution.py:109
  8.7 145.7 %all-gather.13.cloned.1.call-start = ((), (), s32[]{:S(2)}) async-start(), calls=%async_computation.3 | async-start | bytes 2228224 | tf_op jit(solution)/shard_map/all_gather | solution.py:110
  9.3 187.4 %all-gather.21.cloned.1.call-start = ((), (), s32[]{:S(2)}) async-start(), calls=%async_computation.7 | async-start | bytes 2228224 | tf_op jit(solution)/shard_map/all_gather | solution.py:122
  11.0 227.9 %all-gather.19.cloned.1.call-start = ((), (), s32[]{:S(2)}) async-start(), calls=%async_computation.6 | async-start | bytes 2228224 | tf_op jit(solution)/shard_map/all_gather | solution.py:111
  32.9 79.1 %copy-start.2 = (bf16[256,2048]{1,0:T(8,128)(2,1)S(1)}, bf16[256,2048]{1,0:T(8,128)(2,1)}, u32[]{:S(2)}) copy-start(bf16[256,2048]{1,0:T(8,128)(2,1)} %all-gather.11.cloned.1.call-done) | copy-start | bytes 3145732
  200.6 50.3 %all-to-all-start = ((bf16[512,2,1024]{2,0,1:T(8,128)(2,1)}), bf16[512,2,1024]{2,0,1:T(8,128)(2,1)S(1)}, u32[]{:S(2)}, u32[]{:S(2)}) async-start(bf16[512,2,1024]{2,0,1:T(8,128)(2,1)} %copy.41), calls=%async_computation | async-start | bytes 4194304 | tf_op jit(solution)/shard_map/all_to_all | solution.py:123
  204.4 68.4 %all-gather.23.cloned.1.call-start = ((), (), s32[]{:S(2)}) async-start(), calls=%async_computation.8 | async-start | bytes 1572864 | tf_op jit(solution)/shard_map/all_gather | solution.py:133
  241.7 10.0 %copy-start.1 = (bf16[256,1024]{1,0:T(8,128)(2,1)S(1)}, bf16[256,1024]{1,0:T(8,128)(2,1)}, u32[]{:S(2)}) copy-start(bf16[256,1024]{1,0:T(8,128)(2,1)} %param.16) | copy-start | bytes 1572868
  251.7 3.1 copy-start.4
  252.7 116.5 %all-gather.25.cloned.1.call-start = ((), (), s32[]{:S(2)}) async-start(), calls=%async_computation.9 | async-start | bytes 12255232 | tf_op jit(solution)/shard_map/all_gather | solution.py:140
  253.4 210.2 %all-gather.27.cloned.1.call-start = ((), (), s32[]{:S(2)}) async-start(), calls=%async_computation.10 | async-start | bytes 12255232 | tf_op jit(solution)/shard_map/all_gather | solution.py:141
  254.2 306.7 %all-gather.29.cloned.1.call-start = ((), (), s32[]{:S(2)}) async-start(), calls=%async_computation.11 | async-start | bytes 12255232 | tf_op jit(solution)/shard_map/all_gather | solution.py:147
  254.7 340.5 %reduce-scatter.2.cloned.1.call-start = ((), (), s32[]{:S(2)}) async-start(), calls=%async_computation.12 | async-start | bytes 1572864 | tf_op jit(solution)/shard_map/reduce_scatter | solution.py:150
  274.3 286.5 %copy-start.3 = (bf16[256,2048]{1,0:T(8,128)(2,1)S(1)}, bf16[256,2048]{1,0:T(8,128)(2,1)}, u32[]{:S(2)}) copy-start(bf16[256,2048]{1,0:T(8,128)(2,1)} %all-gather.23.cloned.1.call-done) | copy-start | bytes 3145732
  378.6 197.9 %copy-start.5 = (bf16[1024]{0:T(1024)(128)(2,1)S(1)}, bf16[1024]{0:T(1024)(128)(2,1)}, u32[]{:S(2)}) copy-start(bf16[1024]{0:T(1024)(128)(2,1)} %param.29) | copy-start | bytes 6148
  378.6 216.6 %copy-start = (bf16[256,1024]{1,0:T(8,128)(2,1)S(1)}, bf16[256,1024]{1,0:T(8,128)(2,1)}, u32[]{:S(2)}) copy-start(bf16[256,1024]{1,0:T(8,128)(2,1)} %add_convert_fusion) | copy-start | bytes 1572868
Sparse Core Ops, SparseCore 0:
  8.9 23.9 all-gather.10
  35.1 37.8 all-gather.14
  75.1 36.8 all-gather.16
  114.0 40.4 all-gather.12
  156.5 40.1 all-gather.20
  198.7 40.1 all-gather.18
  252.8 19.9 all-gather.22
  275.1 93.9 all-gather.24
  371.4 92.2 all-gather.26
  465.7 95.1 all-gather.28
  576.6 18.5 reduce-scatter.1
where the time goes:
time: 611 us; the launch traced here: 610 us
  waiting for transfers between devices  509 us (83%)
  matrix products  40 us (7%)
  blocking collectives  24.2 us (4%)
  between operations  13.5 us (2%)
  other arithmetic  10.8 us (2%)
  local copies, waits for them, and re-layouts  7.15 us (1%)
    all_gather x1, waiting for transfers between devices, body(): lax.all_gather(ff_down, 'fs', axis=1, tiled=True)  97.2 us
    all_gather x1, waiting for transfers between devices, body(): lax.all_gather(ff_gate, 'fs', axis=0, tiled=True)  94.8 us
    all_gather x1, waiting for transfers between devices, body(): lax.all_gather(ff_up, 'fs', axis=0, tiled=True)  85.1 us
    all_gather x1, waiting for transfers between devices, body(): head_rows = lax.all_gather(out_weight, 'fs', axis=1, tiled=True)  39.8 us
    all_gather x1, waiting for transfers between devices, body(): lax.all_gather(value_weight, 'fs', axis=0, tiled=True)  39.3 us
    all_gather x1, waiting for transfers between devices, body(): lax.all_gather(query_weight, 'fs', axis=0, tiled=True)  38.5 us
    all_gather x1, waiting for transfers between devices, body(): lax.all_gather(key_weight, 'fs', axis=0, tiled=True)  36.8 us
    all_gather x1, waiting for transfers between devices, body(): lax.all_gather(output_gate_weight, 'fs', axis=0, tiled=True)  26.1 us
  transfers between devices with their start and end apart: 12, of which 11 were waited for; matrix products, arithmetic and copies ran while one was open for 6% of the time, Pallas kernels for 0%

commit v1 on v0

--- a/solution.py
+++ b/solution.py
@@ -119,7 +119,12 @@
     normret = retain(query, key, value, head_rates, block_scale)
     gated = (normret * jax.nn.silu(gproj)).astype(jnp.bfloat16)
     all_heads = lax.all_gather(gated, "tp", axis=1, tiled=True)
-    head_rows = lax.all_gather(out_weight, "fs", axis=1, tiled=True)
+    ring = [out_weight]
+    for hop in range(15):
+        ring.append(lax.ppermute(ring[-1], "fs", [(dev, (dev + 1) % 16) for dev in range(16)]))
+    head_rows = jnp.roll(
+        jnp.concatenate(ring[::-1], axis=1), (lax.axis_index("fs") + 1) * ring[0].shape[1], axis=1
+    )
     feature_block = lax.all_to_all(head_rows, "tp", split_axis=1, concat_axis=0, tiled=True)
     width = all_heads.shape[1] // groups
     left = all_heads.reshape(rows, groups, width)

time: 611 us -> 571 us (0.935)
  waiting for transfers between devices: 509 us -> 460 us
    ppermute x0 -> x15, waiting for transfers between devices: none -> 98.9 us  [body(): lax.ppermute(ring[-1], 'fs', [(dev, (dev + 1) % 16) for dev in range(16)])]
    all_gather x1 -> x0, waiting for transfers between devices: 39.8 us -> none  [body(): head_rows = lax.all_gather(out_weight, 'fs', axis=1, tiled=True)]
    all_gather x1, waiting for transfers between devices: 38.5 us -> 0.02 us  [body(): lax.all_gather(query_weight, 'fs', axis=0, tiled=True)]
    all_gather x1, waiting for transfers between devices: 36.8 us -> 0.01 us  [body(): lax.all_gather(key_weight, 'fs', axis=0, tiled=True)]
    all_gather x1, waiting for transfers between devices: 39.3 us -> 20.1 us  [body(): lax.all_gather(value_weight, 'fs', axis=0, tiled=True)]
    all_gather x1, waiting for transfers between devices: 14 us -> 0.01 us  [body(): lax.all_gather(tokens, 'tp', axis=1, tiled=True)]
  transfers between devices with their start and end apart: 12 -> 26, of which waited for: 11 -> 22; matrix products, arithmetic and copies ran while one was open for 6% -> 8% of each run, Pallas kernels for 0% -> 0%
where the time goes in v1:
time: 571 us; the launch traced here: 570 us
  waiting for transfers between devices  460 us (81%)
  matrix products  42.1 us (7%)
  blocking collectives  24.1 us (4%)
  other arithmetic  14 us (2%)
  between operations  14 us (2%)
  local copies, waits for them, and re-layouts  9.6 us (2%)
    ppermute x15, waiting for transfers between devices, body(): lax.ppermute(ring[-1], 'fs', [(dev, (dev + 1) % 16) for dev in range(16)])  98.9 us
    all_gather x1, waiting for transfers between devices, body(): lax.all_gather(ff_down, 'fs', axis=1, tiled=True)  97.3 us
    all_gather x1, waiting for transfers between devices, body(): lax.all_gather(ff_gate, 'fs', axis=0, tiled=True)  94.8 us
    all_gather x1, waiting for transfers between devices, body(): lax.all_gather(ff_up, 'fs', axis=0, tiled=True)  85.1 us
    all_gather x1, waiting for transfers between devices, body(): lax.all_gather(output_gate_weight, 'fs', axis=0, tiled=True)  27.3 us
    all_gather x1, waiting for transfers between devices, body(): lax.all_gather(value_weight, 'fs', axis=0, tiled=True)  20.1 us
    dot_general x5, matrix products, fold_maker(): jnp.dot(source, piece, preferred_element_type=jnp.float32)  19.8 us
    reduce_scatter x1, waiting for transfers between devices, body(): lax.psum_scatter(down_terms.astype(jnp.bfloat16), 'tp', scatter_dimension...  18.7 us
  transfers between devices with their start and end apart: 26, of which 22 were waited for; matrix products, arithmetic and copies ran while one was open for 8% of the time, Pallas kernels for 0%

profile of v1, /device:TPU:0, one launch (start us, length us, event | category | flops | bytes accessed | tf_op | source)
XLA Modules:
  0.0 570.1 jit_solution(11022003330037015834)
XLA Ops:
  9.4 1.0 copy.44
  10.9 7.6 %collective-permute-done = bf16[512,128]{0,1:T(8,128)(2,1)S(1)} collective-permute-done((bf16[512,128]{0,1:T(8,128)(2,1)S(1)}, bf16[512,128]{0,1:T(8,128)(2,1)S(1)}, u32[]{:S(2)}, u32[]{:S(2)}) %collective-permute-start) | collective-permute-done | bytes 131104 | tf_op jit(solution)/shard_map/ppermute | solution.py:124
  18.6 7.1 %collective-permute-done.1 = bf16[512,128]{0,1:T(8,128)(2,1)S(1)} collective-permute-done((bf16[512,128]{0,1:T(8,128)(2,1)S(1)}, bf16[512,128]{0,1:T(8,128)(2,1)S(1)}, u32[]{:S(2)}, u32[]{:S(2)}) %collective-permute-start.1) | collective-permute-done | bytes 131104 | tf_op jit(solution)/shard_map/ppermute | solution.py:124
  25.6 7.1 %collective-permute-done.2 = bf16[512,128]{0,1:T(8,128)(2,1)S(1)} collective-permute-done((bf16[512,128]{0,1:T(8,128)(2,1)S(1)}, bf16[512,128]{0,1:T(8,128)(2,1)S(1)}, u32[]{:S(2)}, u32[]{:S(2)}) %collective-permute-start.2) | collective-permute-done | bytes 131104 | tf_op jit(solution)/shard_map/ppermute | solution.py:124
  32.7 7.1 %collective-permute-done.3 = bf16[512,128]{0,1:T(8,128)(2,1)S(1)} collective-permute-done((bf16[512,128]{0,1:T(8,128)(2,1)S(1)}, bf16[512,128]{0,1:T(8,128)(2,1)S(1)}, u32[]{:S(2)}, u32[]{:S(2)}) %collective-permute-start.3) | collective-permute-done | bytes 131104 | tf_op jit(solution)/shard_map/ppermute | solution.py:124
  39.8 7.2 %collective-permute-done.4 = bf16[512,128]{0,1:T(8,128)(2,1)S(1)} collective-permute-done((bf16[512,128]{0,1:T(8,128)(2,1)S(1)}, bf16[512,128]{0,1:T(8,128)(2,1)S(1)}, u32[]{:S(2)}, u32[]{:S(2)}) %collective-permute-start.4) | collective-permute-done | bytes 131104 | tf_op jit(solution)/shard_map/ppermute | solution.py:124
  47.0 7.5 %collective-permute-done.5 = bf16[512,128]{0,1:T(8,128)(2,1)S(1)} collective-permute-done((bf16[512,128]{0,1:T(8,128)(2,1)S(1)}, bf16[512,128]{0,1:T(8,128)(2,1)S(1)}, u32[]{:S(2)}, u32[]{:S(2)}) %collective-permute-start.5) | collective-permute-done | bytes 131104 | tf_op jit(solution)/shard_map/ppermute | solution.py:124
  54.5 7.1 %collective-permute-done.6 = bf16[512,128]{0,1:T(8,128)(2,1)S(1)} collective-permute-done((bf16[512,128]{0,1:T(8,128)(2,1)S(1)}, bf16[512,128]{0,1:T(8,128)(2,1)S(1)}, u32[]{:S(2)}, u32[]{:S(2)}) %collective-permute-start.6) | collective-permute-done | bytes 131104 | tf_op jit(solution)/shard_map/ppermute | solution.py:124
  61.6 7.7 %collective-permute-done.7 = bf16[512,128]{0,1:T(8,128)(2,1)S(1)} collective-permute-done((bf16[512,128]{0,1:T(8,128)(2,1)S(1)}, bf16[512,128]{0,1:T(8,128)(2,1)S(1)}, u32[]{:S(2)}, u32[]{:S(2)}) %collective-permute-start.7) | collective-permute-done | bytes 131104 | tf_op jit(solution)/shard_map/ppermute | solution.py:124
  70.0 6.4 %collective-permute-done.8 = bf16[512,128]{0,1:T(8,128)(2,1)S(1)} collective-permute-done((bf16[512,128]{0,1:T(8,128)(2,1)S(1)}, bf16[512,128]{0,1:T(8,128)(2,1)S(1)}, u32[]{:S(2)}, u32[]{:S(2)}) %collective-permute-start.8) | collective-permute-done | bytes 131104 | tf_op jit(solution)/shard_map/ppermute | solution.py:124
  76.6 6.9 %collective-permute-done.9 = bf16[512,128]{0,1:T(8,128)(2,1)S(1)} collective-permute-done((bf16[512,128]{0,1:T(8,128)(2,1)S(1)}, bf16[512,128]{0,1:T(8,128)(2,1)S(1)}, u32[]{:S(2)}, u32[]{:S(2)}) %collective-permute-start.9) | collective-permute-done | bytes 131104 | tf_op jit(solution)/shard_map/ppermute | solution.py:124
  83.5 1.3 multiply_exponential_fusion.2
  84.8 6.1 %collective-permute-done.10 = bf16[512,128]{0,1:T(8,128)(2,1)S(1)} collective-permute-done((bf16[512,128]{0,1:T(8,128)(2,1)S(1)}, bf16[512,128]{0,1:T(8,128)(2,1)S(1)}, u32[]{:S(2)}, u32[]{:S(2)}) %collective-permute-start.10) | collective-permute-done | bytes 131104 | tf_op jit(solution)/shard_map/ppermute | solution.py:124
  91.6 6.4 %collective-permute-done.11 = bf16[512,128]{0,1:T(8,128)(2,1)S(1)} collective-permute-done((bf16[512,128]{0,1:T(8,128)(2,1)S(1)}, bf16[512,128]{0,1:T(8,128)(2,1)S(1)}, u32[]{:S(2)}, u32[]{:S(2)}) %collective-permute-start.11) | collective-permute-done | bytes 131104 | tf_op jit(solution)/shard_map/ppermute | solution.py:124
  98.5 5.5 all_gather.37
  104.7 2.0 collective-permute-done.12
  106.7 1.5 fusion.2
  108.2 5.7 collective-permute-done.13
  113.9 7.1 %collective-permute-done.14 = bf16[512,128]{0,1:T(8,128)(2,1)S(1)} collective-permute-done((bf16[512,128]{0,1:T(8,128)(2,1)S(1)}, bf16[512,128]{0,1:T(8,128)(2,1)S(1)}, u32[]{:S(2)}, u32[]{:S(2)}) %collective-permute-start.14) | collective-permute-done | bytes 131104 | tf_op jit(solution)/shard_map/ppermute | solution.py:124
  121.8 2.4 copy.47
  124.2 3.8 all-to-all-start
  128.1 2.6 fusion.50
  130.6 1.9 fusion.48
  132.5 1.0 subtract_bitcast_fusion
  134.3 1.9 convolution_multiply_fusion.1
  136.2 20.1 %all-gather.12.cloned.1.call-done = bf16[2048,512]{1,0:T(8,128)(2,1)} async-done(((bf16[128,512]{1,0:T(8,128)(2,1)}), bf16[2048,512]{1,0:T(8,128)(2,1)}) %all-gather.12.cloned.1.call-update) | async-done | bytes 2097168 | tf_op jit(solution)/shard_map/all_gather | solution.py:110
  156.3 3.1 convolution_convert_fusion.1
  159.4 1.0 reshape.214
  160.8 1.7 fusion.29
  162.5 6.5 %while.13 = (s32[]{:T(128)}, f32[4,64,128]{2,1,0:T(8,128)S(1)}, f32[2,4,64,128]{3,2,1,0:T(8,128)}, f32[2]{0:T(128)}, f32[2,4]{1,0:T(2,128)}, /*index=5*/f32[2,4,...) while((s32[]{:T(128)}, f32[4,64,128]{2,1,0:T(8,128)S(1)}, f32[2,4,64,128]{3,2,1,0:T(8,128)}, ...), condition=%wide.region_2.3_spmd.clone, body=%wide.region_1.2_spmd.clone.sunk | while | flops 196612 | bytes 656572 | solution.py:66
  162.5 1.2 dynamic_slice.30
  165.8 1.2 dynamic_slice.30
  169.0 2.0 multiply_reduce_fusion.1
  171.4 27.3 %all-gather.18.cloned.1.call-done = bf16[2048,512]{1,0:T(8,128)(2,1)} async-done(((bf16[128,512]{1,0:T(8,128)(2,1)}), bf16[2048,512]{1,0:T(8,128)(2,1)}) %all-gather.18.cloned.1.call-update) | async-done | bytes 2097168 | tf_op jit(solution)/shard_map/all_gather | solution.py:111
  198.7 2.8 fusion.16
  201.5 9.1 %all_gather.42 = bf16[256,1024]{1,0:T(8,128)(2,1)S(1)} all-gather(bf16[256,512]{1,0:T(8,128)(2,1)S(1)} %fusion.16), channel_id=1, replica_groups=mesh['fs'=16,'tp'=2] {'tp'}, dimensions={1}, use_global_device_ids=true | all-gather | bytes 786432 | tf_op jit(solution)/shard_map/all_gather | solution.py:121
  214.6 4.5 all_gather.44
  219.1 13.3 %all-gather.20.cloned.1.call-done = bf16[256,2048]{1,0:T(8,128)(2,1)} async-done(((bf16[256,1024]{1,0:T(8,128)(2,1)}), bf16[256,2048]{1,0:T(8,128)(2,1)}) %all-gather.20.cloned.1.call-update) | async-done | bytes 1048592 | tf_op jit(solution)/shard_map/all_gather | solution.py:138
  232.4 1.5 fusion.5
  234.0 94.8 %all-gather.22.cloned.1.call-done = bf16[2048,2816]{1,0:T(8,128)(2,1)} async-done(((bf16[128,2816]{1,0:T(8,128)(2,1)}), bf16[2048,2816]{1,0:T(8,128)(2,1)}) %all-gather.22.cloned.1.call-update) | async-done | bytes 11534352 | tf_op jit(solution)/shard_map/all_gather | solution.py:145
  328.8 9.4 %fusion.21 = f32[256,2816]{1,0:T(8,128)} fusion(bf16[2048,2816]{1,0:T(8,128)(2,1)} %all-gather.22.cloned.1.call-done, bf16[256,2048]{1,0:T(8,128)(2,1)} %all-gather.20.cloned.1.call-done, f32[2048]{0:T(1024)S(1)} %convert_element_type.112, f32[256]{0:T(256)S(1)} %add_rsqrt_fusion.2), kind=kOutput, calls=%fused_computation.35 | convolution fusion | flops 2954887168 | bytes 15475712 | tf_op jit(solution)/shard_map/dot_general | solution.py:77
  338.2 85.1 %all-gather.24.cloned.1.call-done = bf16[2048,2816]{1,0:T(8,128)(2,1)} async-done(((bf16[128,2816]{1,0:T(8,128)(2,1)}), bf16[2048,2816]{1,0:T(8,128)(2,1)}) %all-gather.24.cloned.1.call-update) | async-done | bytes 11534352 | tf_op jit(solution)/shard_map/all_gather | solution.py:146
  423.3 97.3 %all-gather.26.cloned.1.call-done = bf16[2816,2048]{1,0:T(8,128)(2,1)} async-done(((bf16[2816,128]{1,0:T(8,128)(2,1)}), bf16[2816,2048]{1,0:T(8,128)(2,1)}) %all-gather.26.cloned.1.call-update) | async-done | bytes 11534352 | tf_op jit(solution)/shard_map/all_gather | solution.py:152
  520.6 15.6 %convolution_convert_fusion = bf16[256,2048]{1,0:T(8,128)(2,1)} fusion(bf16[2816,2048]{1,0:T(8,128)(2,1)} %all-gather.26.cloned.1.call-done, bf16[2048,2816]{1,0:T(8,128)(2,1)} %all-gather.24.cloned.1.call-done, f32[256,2816]{1,0:T(8,128)} %fusion.21, bf16[256,2048]{1,0:T(8,128)(2,1)S(1)} %copy-done.3, f32[2048]{0:T(1024)S(1)} %convert_element_type.112, ...), kind=kOutput, calls=%fused_computation.11 | convolution fusion | flops 5912526848 | bytes 28058624 | tf_op jit(solution)/shard_map/dot_general | solution.py:150
  536.3 18.7 %reduce-scatter.2.cloned.1.call-done = bf16[256,1024]{1,0:T(8,128)(2,1)} async-done(((bf16[256,2048]{1,0:T(8,128)(2,1)}), bf16[256,1024]{1,0:T(8,128)(2,1)}) %reduce-scatter.2.cloned.1.call-update) | async-done | bytes 524304 | tf_op jit(solution)/shard_map/reduce_scatter | solution.py:155
  555.0 1.3 multiply_reduce_fusion
  556.3 4.9 psum.7
  561.2 2.0 multiply_convert_fusion
  (124 shorter events, 14.8 us)
Async XLA Ops:
  6.5 100.2 %all-gather.10.cloned.1.call-start = ((), (), s32[]{:S(2)}) async-start(), calls=%async_computation.2 | async-start | bytes 1572864 | tf_op jit(solution)/shard_map/all_gather | solution.py:101
  7.3 120.8 %all-gather.14.cloned.1.call-start = ((), (), s32[]{:S(2)}) async-start(), calls=%async_computation.4 | async-start | bytes 1114112 | tf_op jit(solution)/shard_map/all_gather | solution.py:108
  8.0 122.6 %all-gather.16.cloned.1.call-start = ((), (), s32[]{:S(2)}) async-start(), calls=%async_computation.5 | async-start | bytes 1114112 | tf_op jit(solution)/shard_map/all_gather | solution.py:109
  8.7 147.6 %all-gather.12.cloned.1.call-start = ((), (), s32[]{:S(2)}) async-start(), calls=%async_computation.3 | async-start | bytes 2228224 | tf_op jit(solution)/shard_map/all_gather | solution.py:110
  9.3 189.3 %all-gather.18.cloned.1.call-start = ((), (), s32[]{:S(2)}) async-start(), calls=%async_computation.6 | async-start | bytes 2228224 | tf_op jit(solution)/shard_map/all_gather | solution.py:111
  10.4 8.2 %collective-permute-start = (bf16[512,128]{0,1:T(8,128)(2,1)S(1)}, bf16[512,128]{0,1:T(8,128)(2,1)S(1)}, u32[]{:S(2)}, u32[]{:S(2)}) collective-permute-start(bf16[512,128]{0,1:T(8,128)(2,1)S(1)} %copy.44), channel_id=1, source_target_pairs={{0,2},{2,4},{4,6},{6,8},{8,10},{10,12},{12,14},{14,16},{16,18},{18... | collective-permute-start | bytes 393224 | tf_op jit(solution)/shard_map/ppermute | solution.py:124
  18.6 7.1 %collective-permute-start.1 = (bf16[512,128]{0,1:T(8,128)(2,1)S(1)}, bf16[512,128]{0,1:T(8,128)(2,1)S(1)}, u32[]{:S(2)}, u32[]{:S(2)}) collective-permute-start(bf16[512,128]{0,1:T(8,128)(2,1)S(1)} %collective-permute-done), channel_id=1, source_target_pairs={{0,2},{2,4},{4,6},{6,8},{8,10},{10,12},{12,14},{14,16},{16,18},{18... | collective-permute-start | bytes 393224 | tf_op jit(solution)/shard_map/ppermute | solution.py:124
  25.6 7.1 %collective-permute-start.2 = (bf16[512,128]{0,1:T(8,128)(2,1)S(1)}, bf16[512,128]{0,1:T(8,128)(2,1)S(1)}, u32[]{:S(2)}, u32[]{:S(2)}) collective-permute-start(bf16[512,128]{0,1:T(8,128)(2,1)S(1)} %collective-permute-done.1), channel_id=1, source_target_pairs={{0,2},{2,4},{4,6},{6,8},{8,10},{10,12},{12,14},{14,16},{16,18},{18... | collective-permute-start | bytes 393224 | tf_op jit(solution)/shard_map/ppermute | solution.py:124
  32.7 7.1 %collective-permute-start.3 = (bf16[512,128]{0,1:T(8,128)(2,1)S(1)}, bf16[512,128]{0,1:T(8,128)(2,1)S(1)}, u32[]{:S(2)}, u32[]{:S(2)}) collective-permute-start(bf16[512,128]{0,1:T(8,128)(2,1)S(1)} %collective-permute-done.2), channel_id=1, source_target_pairs={{0,2},{2,4},{4,6},{6,8},{8,10},{10,12},{12,14},{14,16},{16,18},{18... | collective-permute-start | bytes 393224 | tf_op jit(solution)/shard_map/ppermute | solution.py:124
  39.8 7.2 %collective-permute-start.4 = (bf16[512,128]{0,1:T(8,128)(2,1)S(1)}, bf16[512,128]{0,1:T(8,128)(2,1)S(1)}, u32[]{:S(2)}, u32[]{:S(2)}) collective-permute-start(bf16[512,128]{0,1:T(8,128)(2,1)S(1)} %collective-permute-done.3), channel_id=1, source_target_pairs={{0,2},{2,4},{4,6},{6,8},{8,10},{10,12},{12,14},{14,16},{16,18},{18... | collective-permute-start | bytes 393224 | tf_op jit(solution)/shard_map/ppermute | solution.py:124
  47.0 7.5 %collective-permute-start.5 = (bf16[512,128]{0,1:T(8,128)(2,1)S(1)}, bf16[512,128]{0,1:T(8,128)(2,1)S(1)}, u32[]{:S(2)}, u32[]{:S(2)}) collective-permute-start(bf16[512,128]{0,1:T(8,128)(2,1)S(1)} %collective-permute-done.4), channel_id=1, source_target_pairs={{0,2},{2,4},{4,6},{6,8},{8,10},{10,12},{12,14},{14,16},{16,18},{18... | collective-permute-start | bytes 393224 | tf_op jit(solution)/shard_map/ppermute | solution.py:124
  54.5 7.1 %collective-permute-start.6 = (bf16[512,128]{0,1:T(8,128)(2,1)S(1)}, bf16[512,128]{0,1:T(8,128)(2,1)S(1)}, u32[]{:S(2)}, u32[]{:S(2)}) collective-permute-start(bf16[512,128]{0,1:T(8,128)(2,1)S(1)} %collective-permute-done.5), channel_id=1, source_target_pairs={{0,2},{2,4},{4,6},{6,8},{8,10},{10,12},{12,14},{14,16},{16,18},{18... | collective-permute-start | bytes 393224 | tf_op jit(solution)/shard_map/ppermute | solution.py:124
  61.6 7.7 %collective-permute-start.7 = (bf16[512,128]{0,1:T(8,128)(2,1)S(1)}, bf16[512,128]{0,1:T(8,128)(2,1)S(1)}, u32[]{:S(2)}, u32[]{:S(2)}) collective-permute-start(bf16[512,128]{0,1:T(8,128)(2,1)S(1)} %collective-permute-done.6), channel_id=1, source_target_pairs={{0,2},{2,4},{4,6},{6,8},{8,10},{10,12},{12,14},{14,16},{16,18},{18... | collective-permute-start | bytes 393224 | tf_op jit(solution)/shard_map/ppermute | solution.py:124
  69.3 7.1 %collective-permute-start.8 = (bf16[512,128]{0,1:T(8,128)(2,1)S(1)}, bf16[512,128]{0,1:T(8,128)(2,1)S(1)}, u32[]{:S(2)}, u32[]{:S(2)}) collective-permute-start(bf16[512,128]{0,1:T(8,128)(2,1)S(1)} %collective-permute-done.7), channel_id=1, source_target_pairs={{0,2},{2,4},{4,6},{6,8},{8,10},{10,12},{12,14},{14,16},{16,18},{18... | collective-permute-start | bytes 393224 | tf_op jit(solution)/shard_map/ppermute | solution.py:124
  76.4 7.1 %collective-permute-start.9 = (bf16[512,128]{0,1:T(8,128)(2,1)S(1)}, bf16[512,128]{0,1:T(8,128)(2,1)S(1)}, u32[]{:S(2)}, u32[]{:S(2)}) collective-permute-start(bf16[512,128]{0,1:T(8,128)(2,1)S(1)} %collective-permute-done.8), channel_id=1, source_target_pairs={{0,2},{2,4},{4,6},{6,8},{8,10},{10,12},{12,14},{14,16},{16,18},{18... | collective-permute-start | bytes 393224 | tf_op jit(solution)/shard_map/ppermute | solution.py:124
  83.5 7.4 %collective-permute-start.10 = (bf16[512,128]{0,1:T(8,128)(2,1)S(1)}, bf16[512,128]{0,1:T(8,128)(2,1)S(1)}, u32[]{:S(2)}, u32[]{:S(2)}) collective-permute-start(bf16[512,128]{0,1:T(8,128)(2,1)S(1)} %collective-permute-done.9), channel_id=1, source_target_pairs={{0,2},{2,4},{4,6},{6,8},{8,10},{10,12},{12,14},{14,16},{16,18},{18... | collective-permute-start | bytes 393224 | tf_op jit(solution)/shard_map/ppermute | solution.py:124
  84.8 13.7 %copy-start.5 = (f32[2,4]{1,0:T(2,128)}, f32[2,4]{1,0:T(2,128)S(1)}, u32[]{:S(2)}) copy-start(f32[2,4]{1,0:T(2,128)S(1)} %get-tuple-element.82) | copy-start | bytes 100
  90.9 7.1 %collective-permute-start.11 = (bf16[512,128]{0,1:T(8,128)(2,1)S(1)}, bf16[512,128]{0,1:T(8,128)(2,1)S(1)}, u32[]{:S(2)}, u32[]{:S(2)}) collective-permute-start(bf16[512,128]{0,1:T(8,128)(2,1)S(1)} %collective-permute-done.10), channel_id=1, source_target_pairs={{0,2},{2,4},{4,6},{6,8},{8,10},{10,12},{12,14},{14,16},{16,18},{18... | collective-permute-start | bytes 393224 | tf_op jit(solution)/shard_map/ppermute | solution.py:124
  98.0 8.7 %collective-permute-start.12 = (bf16[512,128]{0,1:T(8,128)(2,1)S(1)}, bf16[512,128]{0,1:T(8,128)(2,1)S(1)}, u32[]{:S(2)}, u32[]{:S(2)}) collective-permute-start(bf16[512,128]{0,1:T(8,128)(2,1)S(1)} %collective-permute-done.11), channel_id=1, source_target_pairs={{0,2},{2,4},{4,6},{6,8},{8,10},{10,12},{12,14},{14,16},{16,18},{18... | collective-permute-start | bytes 393224 | tf_op jit(solution)/shard_map/ppermute | solution.py:124
  106.7 7.2 %collective-permute-start.13 = (bf16[512,128]{0,1:T(8,128)(2,1)S(1)}, bf16[512,128]{0,1:T(8,128)(2,1)S(1)}, u32[]{:S(2)}, u32[]{:S(2)}) collective-permute-start(bf16[512,128]{0,1:T(8,128)(2,1)S(1)} %collective-permute-done.12), channel_id=1, source_target_pairs={{0,2},{2,4},{4,6},{6,8},{8,10},{10,12},{12,14},{14,16},{16,18},{18... | collective-permute-start | bytes 393224 | tf_op jit(solution)/shard_map/ppermute | solution.py:124
  113.9 7.1 %collective-permute-start.14 = (bf16[512,128]{0,1:T(8,128)(2,1)S(1)}, bf16[512,128]{0,1:T(8,128)(2,1)S(1)}, u32[]{:S(2)}, u32[]{:S(2)}) collective-permute-start(bf16[512,128]{0,1:T(8,128)(2,1)S(1)} %collective-permute-done.13), channel_id=1, source_target_pairs={{0,2},{2,4},{4,6},{6,8},{8,10},{10,12},{12,14},{14,16},{16,18},{18... | collective-permute-start | bytes 393224 | tf_op jit(solution)/shard_map/ppermute | solution.py:124
  113.9 16.7 %copy-start.8 = (f32[256]{0:T(256)}, f32[256]{0:T(256)S(1)}, u32[]{:S(2)}) copy-start(f32[256]{0:T(256)S(1)} %add_rsqrt_fusion.3) | copy-start | bytes 3076
  121.8 6.3 %copy-start.2 = (bf16[256,2048]{1,0:T(8,128)(2,1)S(1)}, bf16[256,2048]{1,0:T(8,128)(2,1)}, u32[]{:S(2)}) copy-start(bf16[256,2048]{1,0:T(8,128)(2,1)} %all-gather.10.cloned.1.call-done) | copy-start | bytes 3145732
  124.2 86.4 %all-to-all-start = ((bf16[512,2,1024]{2,0,1:T(8,128)(2,1)}), bf16[512,2,1024]{2,0,1:T(8,128)(2,1)S(1)}, u32[]{:S(2)}, u32[]{:S(2)}) async-start(bf16[512,2,1024]{2,0,1:T(8,128)(2,1)} %copy.47), calls=%async_computation | async-start | bytes 4194304 | tf_op jit(solution)/shard_map/all_to_all | solution.py:128
  128.0 104.5 %all-gather.20.cloned.1.call-start = ((), (), s32[]{:S(2)}) async-start(), calls=%async_computation.7 | async-start | bytes 1572864 | tf_op jit(solution)/shard_map/all_gather | solution.py:138
  133.6 0.7 copy-start.4
  160.7 37.9 %copy-start.9 = (f32[256]{0:T(256)S(1)}, f32[256]{0:T(256)}, u32[]{:S(2)}) copy-start(f32[256]{0:T(256)} %copy-done.8) | copy-start | bytes 3076
  198.7 12.6 %copy-start.1 = (bf16[256,1024]{1,0:T(8,128)(2,1)S(1)}, bf16[256,1024]{1,0:T(8,128)(2,1)}, u32[]{:S(2)}) copy-start(bf16[256,1024]{1,0:T(8,128)(2,1)} %param.16) | copy-start | bytes 1572868
  210.6 4.0 copy-start.6
  212.3 116.5 %all-gather.22.cloned.1.call-start = ((), (), s32[]{:S(2)}) async-start(), calls=%async_computation.8 | async-start | bytes 12255232 | tf_op jit(solution)/shard_map/all_gather | solution.py:145
  213.0 210.2 %all-gather.24.cloned.1.call-start = ((), (), s32[]{:S(2)}) async-start(), calls=%async_computation.9 | async-start | bytes 12255232 | tf_op jit(solution)/shard_map/all_gather | solution.py:146
  213.8 306.8 %all-gather.26.cloned.1.call-start = ((), (), s32[]{:S(2)}) async-start(), calls=%async_computation.10 | async-start | bytes 12255232 | tf_op jit(solution)/shard_map/all_gather | solution.py:152
  214.5 340.5 %reduce-scatter.2.cloned.1.call-start = ((), (), s32[]{:S(2)}) async-start(), calls=%async_computation.11 | async-start | bytes 1572864 | tf_op jit(solution)/shard_map/reduce_scatter | solution.py:155
  234.0 286.7 %copy-start.3 = (bf16[256,2048]{1,0:T(8,128)(2,1)S(1)}, bf16[256,2048]{1,0:T(8,128)(2,1)}, u32[]{:S(2)}) copy-start(bf16[256,2048]{1,0:T(8,128)(2,1)} %all-gather.20.cloned.1.call-done) | copy-start | bytes 3145732
  338.2 198.1 %copy-start.7 = (bf16[1024]{0:T(1024)(128)(2,1)S(1)}, bf16[1024]{0:T(1024)(128)(2,1)}, u32[]{:S(2)}) copy-start(bf16[1024]{0:T(1024)(128)(2,1)} %param.29) | copy-start | bytes 6148
  338.2 216.8 %copy-start = (bf16[256,1024]{1,0:T(8,128)(2,1)S(1)}, bf16[256,1024]{1,0:T(8,128)(2,1)}, u32[]{:S(2)}) copy-start(bf16[256,1024]{1,0:T(8,128)(2,1)} %add_convert_fusion) | copy-start | bytes 1572868
Sparse Core Ops, SparseCore 0:
  8.9 23.9 all-gather.9
  35.1 37.9 all-gather.13
  75.3 38.1 all-gather.15
  115.5 40.7 all-gather.11
  158.3 40.2 all-gather.17
  212.4 19.9 all-gather.19
  234.7 93.9 all-gather.21
  331.0 92.2 all-gather.23
  425.4 95.1 all-gather.25
  536.4 18.5 reduce-scatter.1
